TPU v7x, 32 devices: a whole 2x2x4 slice. The times are simulated.
32 devices in a mesh: sp: 16 (over z, y, x), tp: 2 (over core).
Axes of the slice: x: 2, y: 2, z: 4, core: 2. Of those that a mesh axis runs over, the one named last changes fastest.
Arguments:
- queries: bfloat16 [8192, 1024], P('sp', 'tp'), may hold values from -8 to 8
- key_rows: bfloat16 [8192, 512], P('sp', 'tp'), may hold values from -8 to 8
- values: bfloat16 [8192, 512], P('sp', 'tp'), may hold values from -16 to 16
- doc_ids: int32 [8192], P('sp'), may hold values from 0 to 7, never falling along the last dimension, each value on 1 to 2048 neighbouring positions
- sink_logits: float32 [16], P('tp'), may hold values from 2.5 to 6
- residual: bfloat16 [8192, 2048], P('sp'), may hold values from -6 to 6
- out_weight: bfloat16 [1024, 2048], P('tp'), may hold values from -0.1875 to 0.1875
- norm_gain: float32 [2048], replicated, may hold values from 0.1 to 1.9
- w_gate: bfloat16 [2048, 5632], P('sp', 'tp'), may hold values from -0.125 to 0.125
- w_up: bfloat16 [2048, 5632], P('sp', 'tp'), may hold values from -0.125 to 0.125
- w_down: bfloat16 [5632, 2048], P('tp', 'sp'), may hold values from -0.078125 to 0.078125
Outputs:
- layer_out: bfloat16 [8192, 2048], P('sp')
Inputs may be any that keep to these rules, and one draw needn't show every extreme that they name: `doc_ids`: document numbers never fall along the positions; each document has 1 to 2048 positions.
All inputs are finite; a program needn't handle non-finite values.
Results may differ from a plain program's by a relative error of at most 0.014.
Values may be sent and summed in bfloat16 or wider, within the bound.
A program may use at most 128 MiB of HBM per device.

v0:
```python
import jax
import jax.numpy as jnp
from jax import lax
from jax.sharding import PartitionSpec as P

HD = 64
WINDOW = 128


def from_behind(shard, axis, by):
    size = lax.axis_size(axis)
    pairs = [(i, i + by) for i in range(size) if 0 <= i + by < size]
    return lax.ppermute(shard, axis, pairs)


def rms_norm(stream, norm_gain):
    floats = stream.astype(jnp.float32)
    scale = lax.rsqrt(jnp.mean(floats * floats, axis=-1, keepdims=True) + 1e-06)
    return floats * scale * norm_gain


def band_rows(tensor, blocks):
    tensor = tensor.reshape((blocks + 1, WINDOW) + tensor.shape[1:])
    return jnp.concatenate([tensor[:-1], tensor[1:]], axis=1)


def attend(queries, key_rows, values, doc_ids, sink_logits):
    local_rows = queries.shape[0]
    blocks = local_rows // WINDOW
    kv_local = key_rows.shape[1] // HD
    per_kv = queries.shape[1] // key_rows.shape[1]
    tail_docs = doc_ids[local_rows - WINDOW :] + 1
    prev_keys, prev_values, prev_docs = from_behind(
        (key_rows[local_rows - WINDOW :], values[local_rows - WINDOW :], tail_docs), "sp", 1
    )
    key_band = band_rows(jnp.concatenate([prev_keys, key_rows], axis=0), blocks).reshape(
        blocks, 2 * WINDOW, kv_local, HD
    )
    value_band = band_rows(jnp.concatenate([prev_values, values], axis=0), blocks).reshape(
        blocks, 2 * WINDOW, kv_local, HD
    )
    doc_band = band_rows(jnp.concatenate([prev_docs - 1, doc_ids]), blocks)
    query_band = queries.reshape(blocks, WINDOW, kv_local, per_kv, HD)
    scores = jnp.einsum(
        "nqhgd,nkhd->nhgqk", query_band, key_band, preferred_element_type=jnp.float32
    ) * HD ** (-0.5)
    offsets = jnp.arange(WINDOW)[:, None] + WINDOW - jnp.arange(2 * WINDOW)[None, :]
    inside = (offsets >= 0) & (offsets < WINDOW)
    query_docs = doc_ids.reshape(blocks, WINDOW)
    allowed = inside[None] & (query_docs[:, :, None] == doc_band[:, None, :])
    scores = jnp.where(allowed[:, None, None], scores, -1e30)
    sink_logit = sink_logits.reshape(kv_local, per_kv)[None, :, :, None, None]
    peak = jnp.maximum(jnp.max(scores, axis=-1, keepdims=True), sink_logit)
    raised = jnp.exp(scores - peak)
    denom = jnp.sum(raised, axis=-1, keepdims=True) + jnp.exp(sink_logit - peak)
    weights = (raised / denom).astype(jnp.bfloat16)
    attended = jnp.einsum(
        "nhgqk,nkhd->nqhgd", weights, value_band, preferred_element_type=jnp.float32
    )
    return attended.astype(jnp.bfloat16).reshape(local_rows, queries.shape[1])


def on_device(
    queries,
    key_rows,
    values,
    doc_ids,
    sink_logits,
    residual,
    out_weight,
    norm_gain,
    w_gate,
    w_up,
    w_down,
):
    attended = attend(queries, key_rows, values, doc_ids, sink_logits)
    mix_term = jnp.dot(attended, out_weight, preferred_element_type=jnp.float32)
    mixed_sum = lax.psum(mix_term.astype(jnp.bfloat16), "tp").astype(jnp.float32)
    stream = (residual.astype(jnp.float32) + mixed_sum).astype(jnp.bfloat16)
    normed = rms_norm(stream, norm_gain).astype(jnp.bfloat16)
    gate_act = jnp.dot(
        normed, lax.all_gather(w_gate, "sp", axis=0, tiled=True), preferred_element_type=jnp.float32
    )
    up_act = jnp.dot(
        normed, lax.all_gather(w_up, "sp", axis=0, tiled=True), preferred_element_type=jnp.float32
    )
    down_whole = lax.all_gather(w_down, "sp", axis=1, tiled=True)
    hidden = (jax.nn.silu(gate_act) * up_act).astype(jnp.bfloat16)
    mlp_term = jnp.dot(hidden, down_whole, preferred_element_type=jnp.float32)
    mlp_total = lax.psum(mlp_term.astype(jnp.bfloat16), "tp").astype(jnp.float32)
    return (stream.astype(jnp.float32) + mlp_total).astype(jnp.bfloat16)


def solution(mesh):
    in_specs = (
        P("sp", "tp"),
        P("sp", "tp"),
        P("sp", "tp"),
        P("sp"),
        P("tp"),
        P("sp", None),
        P("tp", None),
        P(),
        P("sp", "tp"),
        P("sp", "tp"),
        P("tp", "sp"),
    )
    out_specs = P("sp", None)
    return jax.shard_map(
        on_device, mesh=mesh, in_specs=in_specs, out_specs=out_specs, check_vma=False
    )
```

profile of v0, /device:TPU:0, one launch (start us, length us, event | category | flops | bytes accessed | tf_op | source)
XLA Modules:
  0.0 568.8 jit_solution(13624811443397868675)
XLA Ops:
  7.4 0.8 slice_add_fusion
  8.3 4.9 collective-permute-start.1
  13.1 1.5 slice.44
  14.6 4.0 collective-permute-start.2
  18.6 1.5 slice.39
  20.1 2.8 collective-permute-start
  22.9 1.2 reshape.99
  24.1 1.2 reshape.97
  25.4 3.5 reshape.100
  28.9 0.9 copy.21
  29.9 0.9 copy.17
  31.1 0.9 pad_maximum_fusion
  32.2 0.3 copy.20
  32.5 2.2 fusion.5
  34.9 1.9 copy-done.3
  36.7 1.0 fusion.4
  38.1 0.3 copy.16
  38.4 3.4 fusion.8
  41.8 0.4 copy.25
  42.2 2.6 convolution_convert_fusion.1
  44.9 0.5 all-gather.4.cloned.1.call-update
  45.5 0.5 all-gather.6.cloned.1.call-update
  46.1 0.5 all-gather.8.cloned.1.call-update
  46.8 19.7 %all-reduce.3.cloned.1.call-done = bf16[512,2048]{1,0:T(8,128)(2,1)} async-done(((bf16[512,2048]{1,0:T(8,128)(2,1)}), bf16[512,2048]{1,0:T(8,128)(2,1)}) %all-reduce.3.cloned.1.call-update) | async-done | bytes 2097168 | tf_op jit(solution)/shard_map/psum | solution.py:78
  66.5 3.2 fusion
  69.8 119.8 %all-gather.4.cloned.1.call-done = bf16[2048,2816]{1,0:T(8,128)(2,1)} async-done(((bf16[128,2816]{1,0:T(8,128)(2,1)}), bf16[2048,2816]{1,0:T(8,128)(2,1)}) %all-gather.4.cloned.1.call-update) | async-done | bytes 11534352 | tf_op jit(solution)/shard_map/all_gather | solution.py:82
  189.5 11.1 %fusion.13 = f32[512,2816]{1,0:T(8,128)} fusion(bf16[2048,2816]{1,0:T(8,128)(2,1)} %all-gather.4.cloned.1.call-done, bf16[512,2048]{1,0:T(8,128)(2,1)S(1)} %get-tuple-element.6, f32[2048]{0:T(1024)S(1)} %copy-done.9, f32[512]{0:T(512)S(1)} %add_rsqrt_fusion), kind=kOutput, calls=%fused_computation.21 | convolution fusion | flops 5909774336 | bytes 19408896 | tf_op jit(solution)/shard_map/dot_general | solution.py:81
  200.7 130.9 %all-gather.6.cloned.1.call-done = bf16[2048,2816]{1,0:T(8,128)(2,1)} async-done(((bf16[128,2816]{1,0:T(8,128)(2,1)}), bf16[2048,2816]{1,0:T(8,128)(2,1)}) %all-gather.6.cloned.1.call-update) | async-done | bytes 11534352 | tf_op jit(solution)/shard_map/all_gather | solution.py:85
  331.6 182.7 %all-gather.8.cloned.1.call-done = bf16[2816,2048]{1,0:T(8,128)(2,1)} async-done(((bf16[2816,128]{1,0:T(8,128)(2,1)}), bf16[2816,2048]{1,0:T(8,128)(2,1)}) %all-gather.8.cloned.1.call-update) | async-done | bytes 11534352 | tf_op jit(solution)/shard_map/all_gather | solution.py:87
  514.2 22.9 %convolution_convert_fusion = bf16[512,2048]{1,0:T(8,128)(2,1)} fusion(bf16[2816,2048]{1,0:T(8,128)(2,1)} %all-gather.8.cloned.1.call-done, f32[512,2816]{1,0:T(8,128)} %fusion.13, bf16[2048,2816]{1,0:T(8,128)(2,1)} %all-gather.6.cloned.1.call-done, bf16[512,2048]{1,0:T(8,128)(2,1)S(1)} %get-tuple-element.6, f32[2048]{0:T(1024)S(1)} %copy-done.9, ...), kind=kOutput, calls=%fused_computation.14 | convolution fusion | flops 11825053696 | bytes 33040384 | tf_op jit(solution)/shard_map/dot_general | solution.py:89
  537.1 19.6 %all-reduce.5.cloned.1.call-done = bf16[512,2048]{1,0:T(8,128)(2,1)} async-done(((bf16[512,2048]{1,0:T(8,128)(2,1)}), bf16[512,2048]{1,0:T(8,128)(2,1)}) %all-reduce.5.cloned.1.call-update) | async-done | bytes 2097168 | tf_op jit(solution)/shard_map/psum | solution.py:90
  556.7 4.4 fusion.3
  (43 shorter events, 1.5 us)
Async XLA Ops:
  7.4 34.8 %copy-start = (bf16[512,2048]{1,0:T(8,128)(2,1)S(1)}, bf16[512,2048]{1,0:T(8,128)(2,1)}, u32[]{:S(2)}) copy-start(bf16[512,2048]{1,0:T(8,128)(2,1)} %param.17) | copy-start | bytes 6291460
  7.4 23.5 %copy-start.7 = (s32[512]{0:T(512)S(1)}, s32[512]{0:T(512)}, u32[]{:S(2)}) copy-start(s32[512]{0:T(512)} %param.14) | copy-start | bytes 6148
  7.4 23.7 %copy-start.4 = (bf16[512,256]{1,0:T(8,128)(2,1)S(1)}, bf16[512,256]{1,0:T(8,128)(2,1)}, u32[]{:S(2)}) copy-start(bf16[512,256]{1,0:T(8,128)(2,1)} %param.12) | copy-start | bytes 786436
  7.4 22.4 %copy-start.8 = (f32[8]{0:T(128)S(1)}, f32[8]{0:T(128)}, u32[]{:S(2)}) copy-start(f32[8]{0:T(128)} %param.15) | copy-start | bytes 100
  7.4 59.2 %all-reduce.3.cloned.1.call-start = ((), (), s32[]{:S(2)}) async-start(), calls=%async_computation | async-start | bytes 4194304 | tf_op jit(solution)/shard_map/psum | solution.py:78
  8.3 22.6 %collective-permute-start.1 = (s32[128]{0:T(128)S(1)}, s32[128]{0:T(128)S(1)}, u32[]{:S(2)}, u32[]{:S(2)}) collective-permute-start(s32[128]{0:T(128)S(1)} %slice_add_fusion), channel_id=1, source_target_pairs={{0,2},{2,4},{4,6},{6,8},{8,10},{10,12},{12,14},{14,16},{16,18},{18... | collective-permute-start | bytes 1544 | tf_op jit(solution)/shard_map/ppermute | solution.py:13
  14.6 16.5 %collective-permute-start.2 = (bf16[128,256]{1,0:T(8,128)(2,1)}, bf16[128,256]{1,0:T(8,128)(2,1)}, u32[]{:S(2)}, u32[]{:S(2)}) collective-permute-start(bf16[128,256]{1,0:T(8,128)(2,1)} %slice.44), channel_id=1, source_target_pairs={{0,2},{2,4},{4,6},{6,8},{8,10},{10,12},{12,14},{14,16},{16,18},{18... | collective-permute-start | bytes 196616 | tf_op jit(solution)/shard_map/ppermute | solution.py:13
  20.1 17.8 %collective-permute-start = (bf16[128,256]{1,0:T(8,128)(2,1)}, bf16[128,256]{1,0:T(8,128)(2,1)S(1)}, u32[]{:S(2)}, u32[]{:S(2)}) collective-permute-start(bf16[128,256]{1,0:T(8,128)(2,1)} %slice.39), channel_id=1, source_target_pairs={{0,2},{2,4},{4,6},{6,8},{8,10},{10,12},{12,14},{14,16},{16,18},{18... | collective-permute-start | bytes 196616 | tf_op jit(solution)/shard_map/ppermute | solution.py:13
  32.5 5.3 copy-start.5
  34.8 2.0 copy-start.3
  34.8 3.6 copy-start.6
  44.8 144.7 %copy-start.9 = (f32[2048]{0:T(1024)S(1)}, f32[2048]{0:T(1024)}, u32[]{:S(2)}) copy-start(f32[2048]{0:T(1024)} %param.18) | copy-start | bytes 24580
  44.9 144.7 %all-gather.4.cloned.1.call-start = ((), (), s32[]{:S(2)}) async-start(), calls=%async_computation.1 | async-start | bytes 12255232 | tf_op jit(solution)/shard_map/all_gather | solution.py:82
  45.4 286.1 %all-gather.6.cloned.1.call-start = ((), (), s32[]{:S(2)}) async-start(), calls=%async_computation.2 | async-start | bytes 12255232 | tf_op jit(solution)/shard_map/all_gather | solution.py:85
  46.0 468.2 %all-gather.8.cloned.1.call-start = ((), (), s32[]{:S(2)}) async-start(), calls=%async_computation.3 | async-start | bytes 12255232 | tf_op jit(solution)/shard_map/all_gather | solution.py:87
  46.6 510.1 %all-reduce.5.cloned.1.call-start = ((), (), s32[]{:S(2)}) async-start(), calls=%async_computation.4 | async-start | bytes 4194304 | tf_op jit(solution)/shard_map/psum | solution.py:90
  69.8 444.5 %copy-start.2 = (bf16[512,2048]{1,0:T(8,128)(2,1)}, bf16[512,2048]{1,0:T(8,128)(2,1)S(1)}, u32[]{:S(2)}) copy-start(bf16[512,2048]{1,0:T(8,128)(2,1)S(1)} %get-tuple-element.6) | copy-start | bytes 6291460
  537.1 24.1 %copy-start.1 = (bf16[512,2048]{1,0:T(8,128)(2,1)S(1)}, bf16[512,2048]{1,0:T(8,128)(2,1)}, u32[]{:S(2)}) copy-start(bf16[512,2048]{1,0:T(8,128)(2,1)} %param.17) | copy-start | bytes 6291460
Sparse Core Ops, SparseCore 0:
  45.0 21.5 all-reduce.2
  537.2 19.4 all-reduce.4
Sparse Core Ops, SparseCore 1:
  48.1 141.4 all-gather.3
  192.2 139.3 all-gather.5
  334.1 180.0 all-gather.7
where the time goes:
time: 569 us
  waiting for transfers between devices  474 us (83%)
  matrix products  42.2 us (7%)
  between operations  15.3 us (3%)
  local copies, waits for them, and re-layouts  14.2 us (2%)
  starting transfers between devices  12 us (2%)
  other arithmetic  10.8 us (2%)
    all_gather x1, waiting for transfers between devices, on_device(): down_whole = lax.all_gather(w_down, 'sp', axis=1, tiled=True)  183 us
    all_gather x1, waiting for transfers between devices, on_device(): lax.all_gather(w_up, 'sp', axis=0, tiled=True)  131 us
    all_gather x1, waiting for transfers between devices, on_device(): lax.all_gather(w_gate, 'sp', axis=0, tiled=True)  120 us
    dot_general x1, matrix products, on_device(): mlp_term = jnp.dot(hidden, down_whole, preferred_element_type=jnp.float32)  22.9 us
    psum x1, waiting for transfers between devices, on_device(): lax.psum(mix_term.astype(jnp.bfloat16), 'tp').astype(jnp.float32)  19.7 us
    psum x1, waiting for transfers between devices, on_device(): lax.psum(mlp_term.astype(jnp.bfloat16), 'tp').astype(jnp.float32)  19.6 us
    ppermute x3, starting transfers between devices, from_behind(): return lax.ppermute(shard, axis, pairs)  11.6 us
  transfers between devices with their start and end apart: 8, of which 5 were waited for; matrix products, arithmetic and copies ran while one was open for 5% of the time, Pallas kernels for 0%

commit v1 on v0

--- a/solution.py
+++ b/solution.py
@@ -5,6 +5,7 @@
 
 HD = 64
 WINDOW = 128
+INNER = 4
 
 
 def from_behind(shard, axis, by):
@@ -60,6 +61,26 @@
     return attended.astype(jnp.bfloat16).reshape(local_rows, queries.shape[1])
 
 
+def swap(shard, axis, by):
+    size = lax.axis_size(axis)
+    return lax.ppermute(shard, axis, [(i, i ^ by) for i in range(size)])
+
+
+def piece_of(tensor, index, axis, pieces):
+    size = tensor.shape[axis] // pieces
+    return lax.dynamic_slice_in_dim(tensor, index * size, size, axis)
+
+
+def in_order(mine, others, place, axis):
+    size = mine.shape[axis]
+    shape = list(mine.shape)
+    shape[axis] = size * (len(others) + 1)
+    whole = jnp.zeros(shape, mine.dtype)
+    for k, shard in enumerate([mine] + others):
+        whole = lax.dynamic_update_slice_in_dim(whole, shard, (place ^ k) * size, axis)
+    return whole
+
+
 def on_device(
     queries,
     key_rows,
@@ -73,22 +94,56 @@
     w_up,
     w_down,
 ):
+    inner = INNER
+    outer = lax.axis_size("sp") // inner
+    tp = lax.axis_size("tp")
+    seat = lax.rem(lax.axis_index("sp"), inner)
+    core = lax.axis_index("tp")
+    columns = [[row + inner * step for step in range(outer)] for row in range(inner)]
+
+    def gate_up_piece(k):
+        return jnp.concatenate(
+            [piece_of(w_gate, seat ^ k, 1, inner), piece_of(w_up, seat ^ k, 1, inner)], axis=1
+        )
+
+    gate_up = in_order(
+        gate_up_piece(0), [swap(gate_up_piece(k), "sp", k) for k in range(1, inner)], seat, 0
+    )
+    gate_up = lax.all_gather(gate_up, "sp", axis=0, tiled=True, axis_index_groups=columns)
+    down = in_order(
+        piece_of(w_down, seat, 0, inner)[None],
+        [swap(piece_of(w_down, seat ^ k, 0, inner), "sp", k)[None] for k in range(1, inner)],
+        seat,
+        0,
+    )
+    down = lax.all_gather(down, "sp", axis=0, tiled=True, axis_index_groups=columns)
+    down = jnp.swapaxes(down, 0, 1).reshape(down.shape[1], -1)
+
     attended = attend(queries, key_rows, values, doc_ids, sink_logits)
-    mix_term = jnp.dot(attended, out_weight, preferred_element_type=jnp.float32)
-    mixed_sum = lax.psum(mix_term.astype(jnp.bfloat16), "tp").astype(jnp.float32)
-    stream = (residual.astype(jnp.float32) + mixed_sum).astype(jnp.bfloat16)
+    mix_term = jnp.dot(attended, out_weight, preferred_element_type=jnp.float32).astype(jnp.bfloat16)
+    mixed_sum = piece_of(mix_term, core, 0, tp).astype(jnp.float32)
+    for k in range(1, tp):
+        mixed_sum += swap(piece_of(mix_term, core ^ k, 0, tp), "tp", k).astype(jnp.float32)
+    stream = (piece_of(residual, core, 0, tp).astype(jnp.float32) + mixed_sum).astype(jnp.bfloat16)
     normed = rms_norm(stream, norm_gain).astype(jnp.bfloat16)
-    gate_act = jnp.dot(
-        normed, lax.all_gather(w_gate, "sp", axis=0, tiled=True), preferred_element_type=jnp.float32
-    )
-    up_act = jnp.dot(
-        normed, lax.all_gather(w_up, "sp", axis=0, tiled=True), preferred_element_type=jnp.float32
-    )
-    down_whole = lax.all_gather(w_down, "sp", axis=1, tiled=True)
-    hidden = (jax.nn.silu(gate_act) * up_act).astype(jnp.bfloat16)
-    mlp_term = jnp.dot(hidden, down_whole, preferred_element_type=jnp.float32)
-    mlp_total = lax.psum(mlp_term.astype(jnp.bfloat16), "tp").astype(jnp.float32)
-    return (stream.astype(jnp.float32) + mlp_total).astype(jnp.bfloat16)
+    rows, width = normed.shape
+    near = jnp.concatenate([normed] + [swap(normed, "sp", k) for k in range(1, inner)], axis=0)
+    tokens = jnp.concatenate([near] + [swap(near, "tp", k) for k in range(1, tp)], axis=0)
+
+    acts = jnp.dot(tokens, gate_up, preferred_element_type=jnp.float32)
+    units = acts.shape[1] // 2
+    hidden = (jax.nn.silu(acts[:, :units]) * acts[:, units:]).astype(jnp.bfloat16)
+    mlp_term = jnp.dot(hidden, down, preferred_element_type=jnp.float32).astype(jnp.bfloat16)
+    mlp_term = mlp_term.reshape(tp, inner * rows, width)
+    near_sum = mlp_term[0].astype(jnp.float32)
+    for k in range(1, tp):
+        near_sum += swap(mlp_term[k], "tp", k).astype(jnp.float32)
+    near_sum = near_sum.reshape(inner, rows, width)
+    total = near_sum[0]
+    for k in range(1, inner):
+        total += swap(near_sum[k].astype(jnp.bfloat16), "sp", k).astype(jnp.float32)
+    out = (stream.astype(jnp.float32) + total).astype(jnp.bfloat16)
+    return in_order(out, [swap(out, "tp", k) for k in range(1, tp)], core, 0)
 
 
 def solution(mesh):

time: 569 us -> 319 us (0.56)
  waiting for transfers between devices: 474 us -> 160 us
  local copies, waits for them, and re-layouts: 14.2 us -> 51 us
  other arithmetic: 10.8 us -> 26.7 us
  starting transfers between devices: 12 us -> 26.6 us
    all_gather x3 -> x2, waiting for transfers between devices: 433 us -> 57 us  [the longest x1 40.2 us: on_device(): lax.all_gather(down, 'sp', axis=0, tiled=True, axis_index_groups=columns)]
    ppermute x0 -> x16, waiting for transfers between devices: none -> 103 us  [swap(): return lax.ppermute(shard, axis, [(i, i ^ by) for i in range(size)])]
    psum x2 -> x0, waiting for transfers between devices: 39.3 us -> none  [the longest x1 19.7 us: on_device(): lax.psum(mix_term.astype(jnp.bfloat16), 'tp').astype(jnp.float32)]
    ppermute x0 -> x16, starting transfers between devices: none -> 14.2 us  [swap(): return lax.ppermute(shard, axis, [(i, i ^ by) for i in range(size)])]
    dynamic_update_slice x0 -> x8, local copies, waits for them, and re-layouts: none -> 10.5 us  [in_order(): lax.dynamic_update_slice_in_dim(whole, shard, (place ^ k) * size, axis)]
    concatenate x8, local copies, waits for them, and re-layouts: 5.36 us -> 14 us  [band_rows(): return jnp.concatenate([tensor[:-1], tensor[1:]], axis=1)]
  transfers between devices with their start and end apart: 8 -> 21, of which waited for: 5 -> 11; matrix products, arithmetic and copies ran while one was open for 5% -> 29% of each run, Pallas kernels for 0% -> 0%
where the time goes in v1:
time: 319 us; the launch traced here: 317 us
  waiting for transfers between devices  160 us (50%)
  local copies, waits for them, and re-layouts  51 us (16%)
  matrix products  39.4 us (12%)
  other arithmetic  26.7 us (8%)
  starting transfers between devices  26.6 us (8%)
  between operations  13.7 us (4%)
    ppermute x16, waiting for transfers between devices, swap(): return lax.ppermute(shard, axis, [(i, i ^ by) for i in range(size)])  103 us
    all_gather x1, waiting for transfers between devices, on_device(): lax.all_gather(down, 'sp', axis=0, tiled=True, axis_index_groups=columns)  40.2 us
    dot_general x1, matrix products, on_device(): acts = jnp.dot(tokens, gate_up, preferred_element_type=jnp.float32)  18.8 us
    all_gather x1, waiting for transfers between devices, on_device(): lax.all_gather(gate_up, 'sp', axis=0, tiled=True, axis_index_groups=columns)  16.8 us
    ppermute x16, starting transfers between devices, swap(): return lax.ppermute(shard, axis, [(i, i ^ by) for i in range(size)])  14.2 us
    concatenate x8, local copies, waits for them, and re-layouts, band_rows(): return jnp.concatenate([tensor[:-1], tensor[1:]], axis=1)  14 us
    ppermute x3, starting transfers between devices, from_behind(): return lax.ppermute(shard, axis, pairs)  12.3 us
    dot_general x1, matrix products, on_device(): jnp.dot(hidden, down, preferred_element_type=jnp.float32)  10.9 us
  transfers between devices with their start and end apart: 21, of which 11 were waited for; matrix products, arithmetic and copies ran while one was open for 29% of the time, Pallas kernels for 0%

profile of v1, /device:TPU:0, one launch (start us, length us, event | category | flops | bytes accessed | tf_op | source)
XLA Modules:
  0.0 317.4 jit_solution(11901778430436596371)
XLA Ops:
  7.4 4.9 %collective-permute-start.1 = (s32[128]{0:T(128)S(1)}, s32[128]{0:T(128)S(1)}, u32[]{:S(2)}, u32[]{:S(2)}) collective-permute-start(s32[128]{0:T(128)S(1)} %slice_add_fusion.1), channel_id=1, source_target_pairs={{0,2},{2,4},{4,6},{6,8},{8,10},{10,12},{12,14},{14,16},{16,18},{18... | collective-permute-start | bytes 1544 | tf_op jit(solution)/shard_map/ppermute | solution.py:14
  13.7 4.0 %collective-permute-start.2 = (bf16[128,256]{1,0:T(8,128)(2,1)}, bf16[128,256]{1,0:T(8,128)(2,1)}, u32[]{:S(2)}, u32[]{:S(2)}) collective-permute-start(bf16[128,256]{1,0:T(8,128)(2,1)} %slice.77), channel_id=1, source_target_pairs={{0,2},{2,4},{4,6},{6,8},{8,10},{10,12},{12,14},{14,16},{16,18},{18... | collective-permute-start | bytes 196616 | tf_op jit(solution)/shard_map/ppermute | solution.py:14
  19.2 3.4 %collective-permute-start = (bf16[128,256]{1,0:T(8,128)(2,1)}, bf16[128,256]{1,0:T(8,128)(2,1)}, u32[]{:S(2)}, u32[]{:S(2)}) collective-permute-start(bf16[128,256]{1,0:T(8,128)(2,1)} %slice.72), channel_id=1, source_target_pairs={{0,2},{2,4},{4,6},{6,8},{8,10},{10,12},{12,14},{14,16},{16,18},{18... | collective-permute-start | bytes 196616 | tf_op jit(solution)/shard_map/ppermute | solution.py:14
  22.6 3.0 constant_dynamic-slice_fusion.3
  34.7 3.5 %reshape.118 = bf16[4,128,4,2,64]{4,3,2,1,0:T(2,128)(2,1)} reshape(bf16[512,512]{1,0:T(8,128)(2,1)} %param.11) | data formatting | bytes 1048576 | tf_op jit(solution)/shard_map/reshape | solution.py:44
  38.2 2.0 copy.52
  40.9 2.0 copy.48
  47.2 2.0 reshape.116
  49.2 1.9 copy.51
  51.1 4.9 %fusion.2 = (f32[4,4,2,128]{3,2,1,0:T(2,128)}, f32[4,4,256,128,2]{3,2,4,1,0:T(8,128)}) fusion(pred[4,128,256]{1,2,0:T(8,128)(4,1)} %compare_and_fusion, bf16[4,128,4,2,64]{4,3,2,1,0:T(2,128)(2,1)} %reshape.118, bf16[4,128,4,64]{1,3,2,0:T(8,128)(2,1)} %copy.52, bf16[4,128,4,64]{1,3,2,0:T(8,128)(2,1)} %copy.51), kind=kOutput, calls=%fused_computation.9 | convolution fusion | flops 138407936 | bytes 5390336 | tf_op jit(solution)/shard_map/nqhgd,nkhd->nhgqk/dot_general | solution.py:45
  57.6 2.0 reshape.114
  59.6 2.0 copy.47
  66.7 3.2 %fusion.1 = f32[4,4,2,128]{3,2,1,0:T(2,128)S(1)} fusion(f32[4,4,256,128,2]{3,2,4,1,0:T(8,128)} %get-tuple-element.28, f32[4,4,2,128]{3,2,1,0:T(2,128)S(1)} %broadcast_maximum_fusion, pred[4,128,256]{1,2,0:T(8,128)(4,1)} %compare_and_fusion), kind=kLoop, calls=%fused_computation.8 | loop fusion | flops 4190208 | bytes 4358144 | tf_op jit(solution)/shard_map/reduce_sum | solution.py:56
  70.2 2.2 fusion.15
  72.9 2.6 convolution_convert_fusion.1
  76.9 2.6 collective-permute-done.3
  79.5 2.2 fusion.7
  86.6 22.5 %collective-permute-done.4 = bf16[256,2048]{1,0:T(8,128)(2,1)S(1)} collective-permute-done((bf16[256,2048]{1,0:T(8,128)(2,1)S(1)}, bf16[256,2048]{1,0:T(8,128)(2,1)S(1)}, u32[]{:S(2)}, u32[]{:S(2)}) %collective-permute-start.4) | collective-permute-done | bytes 1048608 | tf_op jit(solution)/shard_map/ppermute | solution.py:66
  109.1 22.4 %collective-permute-done.5 = bf16[256,2048]{1,0:T(8,128)(2,1)S(1)} collective-permute-done((bf16[256,2048]{1,0:T(8,128)(2,1)S(1)}, bf16[256,2048]{1,0:T(8,128)(2,1)S(1)}, u32[]{:S(2)}, u32[]{:S(2)}) %collective-permute-start.5) | collective-permute-done | bytes 1048608 | tf_op jit(solution)/shard_map/ppermute | solution.py:66
  131.5 2.5 pad_maximum_fusion
  140.8 1.7 collective-permute-done.11
  151.6 4.7 %constant_dynamic-update-slice_fusion = bf16[2048,2048]{1,0:T(8,128)(2,1)} fusion(bf16[2048,2048]{1,0:T(8,128)(2,1)} %constant_dynamic-update-slice_fusion.1, bf16[1024,2048]{1,0:T(8,128)(2,1)} %collective-permute-done.7), kind=kLoop, calls=%fused_computation.54 | loop fusion | bytes 8388608 | tf_op jit(solution)/shard_map/concatenate | solution.py:131
  156.3 16.8 %all-gather.3.cloned.1.call-done = bf16[2048,1408]{1,0:T(8,128)(2,1)} async-done(((bf16[512,1408]{1,0:T(8,128)(2,1)}), bf16[2048,1408]{1,0:T(8,128)(2,1)}) %all-gather.3.cloned.1.call-update) | async-done | bytes 5767184 | tf_op jit(solution)/shard_map/all_gather | solution.py:112
  173.1 18.8 %fusion.36 = f32[2048,1408]{0,1:T(8,128)} fusion(bf16[2048,2048]{1,0:T(8,128)(2,1)} %constant_dynamic-update-slice_fusion, bf16[2048,1408]{1,0:T(8,128)(2,1)} %all-gather.3.cloned.1.call-done), kind=kOutput, calls=%fused_computation.91 | convolution fusion | flops 11811160064 | bytes 25690112 | tf_op jit(solution)/shard_map/dot_general | solution.py:133
  191.9 40.2 %all-gather.5.cloned.1.call-done = bf16[16,704,128]{2,1,0:T(8,128)(2,1)} async-done(((bf16[4,704,128]{2,1,0:T(8,128)(2,1)}), bf16[16,704,128]{2,1,0:T(8,128)(2,1)}) %all-gather.5.cloned.1.call-update) | async-done | bytes 2883600 | tf_op jit(solution)/shard_map/all_gather | solution.py:119
  232.1 10.9 %convolution_convert_fusion = bf16[2048,2048]{1,0:T(8,128)(2,1)S(1)} fusion(f32[2048,1408]{0,1:T(8,128)} %fusion.36, bf16[16,704,128]{2,1,0:T(8,128)(2,1)} %all-gather.5.cloned.1.call-done), kind=kOutput, calls=%fused_computation.1 | convolution fusion | flops 5918425088 | bytes 22806528 | tf_op jit(solution)/shard_map/dot_general | solution.py:136
  243.7 2.6 copy-done.2
  246.3 4.7 %collective-permute-done.14 = bf16[1024,2048]{1,0:T(8,128)(2,1)} collective-permute-done((bf16[1024,2048]{1,0:T(8,128)(2,1)S(1)}, bf16[1024,2048]{1,0:T(8,128)(2,1)}, u32[]{:S(2)}, u32[]{:S(2)}) %collective-permute-start.14) | collective-permute-done | bytes 4194336 | tf_op jit(solution)/shard_map/ppermute | solution.py:66
  250.9 5.6 %convert_add_fusion = (f32[1024,2048]{1,0:T(8,128)S(1)}, bf16[1024,2048]{1,0:T(8,128)(2,1)S(1)}) fusion(bf16[1024,2048]{1,0:T(8,128)(2,1)} %collective-permute-done.14, bf16[2048,2048]{1,0:T(8,128)(2,1)} %copy-done.2), kind=kLoop, calls=%fused_computation | loop fusion | flops 8388608 | bytes 20971520 | tf_op jit(solution)/shard_map/add | solution.py:140
  260.3 22.5 %collective-permute-done.15 = bf16[256,2048]{1,0:T(8,128)(2,1)S(1)} collective-permute-done((bf16[256,2048]{1,0:T(8,128)(2,1)S(1)}, bf16[256,2048]{1,0:T(8,128)(2,1)S(1)}, u32[]{:S(2)}, u32[]{:S(2)}) %collective-permute-start.15) | collective-permute-done | bytes 1048608 | tf_op jit(solution)/shard_map/ppermute | solution.py:66
  282.8 22.8 %collective-permute-done.16 = bf16[256,2048]{1,0:T(8,128)(2,1)S(1)} collective-permute-done((bf16[256,2048]{1,0:T(8,128)(2,1)S(1)}, bf16[256,2048]{1,0:T(8,128)(2,1)S(1)}, u32[]{:S(2)}, u32[]{:S(2)}) %collective-permute-start.16) | collective-permute-done | bytes 1048608 | tf_op jit(solution)/shard_map/ppermute | solution.py:66
  306.9 2.6 collective-permute-done.18
  (109 shorter events, 54.0 us)
Async XLA Ops:
  6.5 66.3 %copy-start = (bf16[512,2048]{1,0:T(8,128)(2,1)S(1)}, bf16[512,2048]{1,0:T(8,128)(2,1)}, u32[]{:S(2)}) copy-start(bf16[512,2048]{1,0:T(8,128)(2,1)} %param.17) | copy-start | bytes 6291460
  6.5 23.3 %copy-start.8 = (bf16[512,256]{1,0:T(8,128)(2,1)S(1)}, bf16[512,256]{1,0:T(8,128)(2,1)}, u32[]{:S(2)}) copy-start(bf16[512,256]{1,0:T(8,128)(2,1)} %param.12) | copy-start | bytes 786436
  6.5 24.4 %copy-start.9 = (bf16[512,256]{1,0:T(8,128)(2,1)S(1)}, bf16[512,256]{1,0:T(8,128)(2,1)}, u32[]{:S(2)}) copy-start(bf16[512,256]{1,0:T(8,128)(2,1)} %param.13) | copy-start | bytes 786436
  6.5 166.6 %all-gather.3.cloned.1.call-start = ((), (), s32[]{:S(2)}) async-start(), calls=%async_computation | async-start | bytes 7208960 | tf_op jit(solution)/shard_map/all_gather | solution.py:112
  7.4 35.4 %collective-permute-start.1 = (s32[128]{0:T(128)S(1)}, s32[128]{0:T(128)S(1)}, u32[]{:S(2)}, u32[]{:S(2)}) collective-permute-start(s32[128]{0:T(128)S(1)} %slice_add_fusion.1), channel_id=1, source_target_pairs={{0,2},{2,4},{4,6},{6,8},{8,10},{10,12},{12,14},{14,16},{16,18},{18... | collective-permute-start | bytes 1544 | tf_op jit(solution)/shard_map/ppermute | solution.py:14
  13.7 31.8 %collective-permute-start.2 = (bf16[128,256]{1,0:T(8,128)(2,1)}, bf16[128,256]{1,0:T(8,128)(2,1)}, u32[]{:S(2)}, u32[]{:S(2)}) collective-permute-start(bf16[128,256]{1,0:T(8,128)(2,1)} %slice.77), channel_id=1, source_target_pairs={{0,2},{2,4},{4,6},{6,8},{8,10},{10,12},{12,14},{14,16},{16,18},{18... | collective-permute-start | bytes 196616 | tf_op jit(solution)/shard_map/ppermute | solution.py:14
  19.2 36.8 %collective-permute-start = (bf16[128,256]{1,0:T(8,128)(2,1)}, bf16[128,256]{1,0:T(8,128)(2,1)}, u32[]{:S(2)}, u32[]{:S(2)}) collective-permute-start(bf16[128,256]{1,0:T(8,128)(2,1)} %slice.72), channel_id=1, source_target_pairs={{0,2},{2,4},{4,6},{6,8},{8,10},{10,12},{12,14},{14,16},{16,18},{18... | collective-permute-start | bytes 196616 | tf_op jit(solution)/shard_map/ppermute | solution.py:14
  25.6 14.6 %copy-start.17 = (f32[8]{0:T(128)S(1)}, f32[8]{0:T(128)}, u32[]{:S(2)}) copy-start(f32[8]{0:T(128)} %param.15) | copy-start | bytes 100
  26.5 35.9 %collective-permute-start.8 = (bf16[128,1408]{1,0:T(8,128)(2,1)}, bf16[128,1408]{1,0:T(8,128)(2,1)}, u32[]{:S(2)}, u32[]{:S(2)}) collective-permute-start(bf16[128,1408]{1,0:T(8,128)(2,1)} %pad_maximum_fusion.1), channel_id=1, source_target_pairs={{0,2},{2,0},{4,6},{6,4},{8,10},{10,8},{12,14},{14,12},{16,18},{18,... | collective-permute-start | bytes 1081352 | tf_op jit(solution)/shard_map/ppermute | solution.py:66
  27.4 16.4 %copy-start.14 = (s32[512]{0:T(512)S(1)}, s32[512]{0:T(512)}, u32[]{:S(2)}) copy-start(s32[512]{0:T(512)} %param.14) | copy-start | bytes 6148
  28.3 35.1 %collective-permute-start.9 = (bf16[128,1408]{1,0:T(8,128)(2,1)}, bf16[128,1408]{1,0:T(8,128)(2,1)}, u32[]{:S(2)}, u32[]{:S(2)}) collective-permute-start(bf16[128,1408]{1,0:T(8,128)(2,1)} %pad_maximum_fusion.2), channel_id=1, source_target_pairs={{0,4},{2,6},{4,0},{6,2},{8,12},{10,14},{12,8},{14,10},{16,20},{18,... | collective-permute-start | bytes 1081352 | tf_op jit(solution)/shard_map/ppermute | solution.py:66
  42.8 21.6 %collective-permute-start.10 = (bf16[128,1408]{1,0:T(8,128)(2,1)}, bf16[128,1408]{1,0:T(8,128)(2,1)}, u32[]{:S(2)}, u32[]{:S(2)}) collective-permute-start(bf16[128,1408]{1,0:T(8,128)(2,1)} %pad_maximum_fusion.3), channel_id=1, source_target_pairs={{0,6},{2,4},{4,2},{6,0},{8,14},{10,12},{12,10},{14,8},{16,22},{18,... | collective-permute-start | bytes 1081352 | tf_op jit(solution)/shard_map/ppermute | solution.py:66
  51.1 4.9 %copy-start.10 = (bf16[512,256]{1,0:T(8,128)(2,1)S(1)}, bf16[512,256]{1,0:T(8,128)(2,1)}, u32[]{:S(2)}) copy-start(bf16[512,256]{1,0:T(8,128)(2,1)} %param.13) | copy-start | bytes 786436
  66.6 3.4 %copy-start.12 = (pred[4,128,256]{1,2,0:T(8,128)(4,1)S(1)}, pred[4,128,256]{1,2,0:T(8,128)(4,1)}, u32[]{:S(2)}) copy-start(pred[4,128,256]{1,2,0:T(8,128)(4,1)} %compare_and_fusion) | copy-start | bytes 393220
  66.7 165.5 %all-gather.5.cloned.1.call-start = ((), (), s32[]{:S(2)}) async-start(), calls=%async_computation.1 | async-start | bytes 3604480 | tf_op jit(solution)/shard_map/all_gather | solution.py:119
  66.7 3.5 %copy-start.4 = (f32[4,4,256,128,2]{3,2,4,1,0:T(8,128)S(1)}, f32[4,4,256,128,2]{3,2,4,1,0:T(8,128)}, u32[]{:S(2)}) copy-start(f32[4,4,256,128,2]{3,2,4,1,0:T(8,128)} %get-tuple-element.28) | copy-start | bytes 12582916
  75.5 6.3 %copy-start.16 = (f32[2048]{0:T(1024)S(1)}, f32[2048]{0:T(1024)}, u32[]{:S(2)}) copy-start(f32[2048]{0:T(1024)} %param.18) | copy-start | bytes 24580
  76.8 2.7 collective-permute-start.3
  83.1 50.9 %copy-start.11 = (bf16[2816,128]{1,0:T(8,128)(2,1)S(1)}, bf16[2816,128]{1,0:T(8,128)(2,1)}, u32[]{:S(2)}) copy-start(bf16[2816,128]{1,0:T(8,128)(2,1)} %param.21) | copy-start | bytes 2162692
  83.1 26.0 %collective-permute-start.4 = (bf16[256,2048]{1,0:T(8,128)(2,1)S(1)}, bf16[256,2048]{1,0:T(8,128)(2,1)S(1)}, u32[]{:S(2)}, u32[]{:S(2)}) collective-permute-start(bf16[256,2048]{1,0:T(8,128)(2,1)S(1)} %get-tuple-element.8), channel_id=1, source_target_pairs={{0,2},{2,0},{4,6},{6,4},{8,10},{10,8},{12,14},{14,12},{16,18},{18,... | collective-permute-start | bytes 3145736 | tf_op jit(solution)/shard_map/ppermute | solution.py:66
  84.1 47.4 %collective-permute-start.5 = (bf16[256,2048]{1,0:T(8,128)(2,1)S(1)}, bf16[256,2048]{1,0:T(8,128)(2,1)S(1)}, u32[]{:S(2)}, u32[]{:S(2)}) collective-permute-start(bf16[256,2048]{1,0:T(8,128)(2,1)S(1)} %get-tuple-element.8), channel_id=1, source_target_pairs={{0,4},{2,6},{4,0},{6,2},{8,12},{10,14},{12,8},{14,10},{16,20},{18,... | collective-permute-start | bytes 3145736 | tf_op jit(solution)/shard_map/ppermute | solution.py:66
  85.6 45.9 %collective-permute-start.6 = (bf16[256,2048]{1,0:T(8,128)(2,1)S(1)}, bf16[256,2048]{1,0:T(8,128)(2,1)S(1)}, u32[]{:S(2)}, u32[]{:S(2)}) collective-permute-start(bf16[256,2048]{1,0:T(8,128)(2,1)S(1)} %get-tuple-element.8), channel_id=1, source_target_pairs={{0,6},{2,4},{4,2},{6,0},{8,14},{10,12},{12,10},{14,8},{16,22},{18,... | collective-permute-start | bytes 3145736 | tf_op jit(solution)/shard_map/ppermute | solution.py:66
  133.9 17.6 %collective-permute-start.7 = (bf16[1024,2048]{1,0:T(8,128)(2,1)}, bf16[1024,2048]{1,0:T(8,128)(2,1)}, u32[]{:S(2)}, u32[]{:S(2)}) collective-permute-start(bf16[1024,2048]{1,0:T(8,128)(2,1)} %pad_maximum_fusion), channel_id=1, source_target_pairs={{0,1},{1,0},{2,3},{3,2},{4,5},{5,4},{6,7},{7,6},{8,9},{9,8},{10,11... | collective-permute-start | bytes 12582920 | tf_op jit(solution)/shard_map/ppermute | solution.py:66
  134.7 7.7 %collective-permute-start.11 = (bf16[704,128]{1,0:T(8,128)(2,1)}, bf16[704,128]{1,0:T(8,128)(2,1)}, u32[]{:S(2)}, u32[]{:S(2)}) collective-permute-start(bf16[704,128]{1,0:T(8,128)(2,1)} %get-tuple-element.17), channel_id=1, source_target_pairs={{0,2},{2,0},{4,6},{6,4},{8,10},{10,8},{12,14},{14,12},{16,18},{18,... | collective-permute-start | bytes 540680 | tf_op jit(solution)/shard_map/ppermute | solution.py:66
  135.9 8.1 %collective-permute-start.12 = (bf16[704,128]{1,0:T(8,128)(2,1)S(1)}, bf16[704,128]{1,0:T(8,128)(2,1)}, u32[]{:S(2)}, u32[]{:S(2)}) collective-permute-start(bf16[704,128]{1,0:T(8,128)(2,1)S(1)} %get-tuple-element.18), channel_id=1, source_target_pairs={{0,4},{2,6},{4,0},{6,2},{8,12},{10,14},{12,8},{14,10},{16,20},{18,... | collective-permute-start | bytes 540680 | tf_op jit(solution)/shard_map/ppermute | solution.py:66
  136.7 10.0 %collective-permute-start.13 = (bf16[704,128]{1,0:T(8,128)(2,1)S(1)}, bf16[704,128]{1,0:T(8,128)(2,1)}, u32[]{:S(2)}, u32[]{:S(2)}) collective-permute-start(bf16[704,128]{1,0:T(8,128)(2,1)S(1)} %get-tuple-element.16), channel_id=1, source_target_pairs={{0,6},{2,4},{4,2},{6,0},{8,14},{10,12},{12,10},{14,8},{16,22},{18,... | collective-permute-start | bytes 540680 | tf_op jit(solution)/shard_map/ppermute | solution.py:66
  243.6 7.4 %collective-permute-start.14 = (bf16[1024,2048]{1,0:T(8,128)(2,1)S(1)}, bf16[1024,2048]{1,0:T(8,128)(2,1)}, u32[]{:S(2)}, u32[]{:S(2)}) collective-permute-start(bf16[1024,2048]{1,0:T(8,128)(2,1)S(1)} %slice.90), channel_id=1, source_target_pairs={{0,1},{1,0},{2,3},{3,2},{4,5},{5,4},{6,7},{7,6},{8,9},{9,8},{10,11... | collective-permute-start | bytes 12582920 | tf_op jit(solution)/shard_map/ppermute | solution.py:66
  256.7 26.1 %collective-permute-start.15 = (bf16[256,2048]{1,0:T(8,128)(2,1)S(1)}, bf16[256,2048]{1,0:T(8,128)(2,1)S(1)}, u32[]{:S(2)}, u32[]{:S(2)}) collective-permute-start(bf16[256,2048]{1,0:T(8,128)(2,1)S(1)} %get-tuple-element.13), channel_id=1, source_target_pairs={{0,2},{2,0},{4,6},{6,4},{8,10},{10,8},{12,14},{14,12},{16,18},{18,... | collective-permute-start | bytes 3145736 | tf_op jit(solution)/shard_map/ppermute | solution.py:66
  258.3 47.4 %collective-permute-start.16 = (bf16[256,2048]{1,0:T(8,128)(2,1)S(1)}, bf16[256,2048]{1,0:T(8,128)(2,1)S(1)}, u32[]{:S(2)}, u32[]{:S(2)}) collective-permute-start(bf16[256,2048]{1,0:T(8,128)(2,1)S(1)} %get-tuple-element.15), channel_id=1, source_target_pairs={{0,4},{2,6},{4,0},{6,2},{8,12},{10,14},{12,8},{14,10},{16,20},{18,... | collective-permute-start | bytes 3145736 | tf_op jit(solution)/shard_map/ppermute | solution.py:66
  259.8 45.9 %collective-permute-start.17 = (bf16[256,2048]{1,0:T(8,128)(2,1)S(1)}, bf16[256,2048]{1,0:T(8,128)(2,1)S(1)}, u32[]{:S(2)}, u32[]{:S(2)}) collective-permute-start(bf16[256,2048]{1,0:T(8,128)(2,1)S(1)} %get-tuple-element.14), channel_id=1, source_target_pairs={{0,6},{2,4},{4,2},{6,0},{8,14},{10,12},{12,10},{14,8},{16,22},{18,... | collective-permute-start | bytes 3145736 | tf_op jit(solution)/shard_map/ppermute | solution.py:66
  305.7 4.9 %copy-start.1 = (bf16[512,2048]{1,0:T(8,128)(2,1)S(1)}, bf16[512,2048]{1,0:T(8,128)(2,1)}, u32[]{:S(2)}) copy-start(bf16[512,2048]{1,0:T(8,128)(2,1)} %param.17) | copy-start | bytes 6291460
  306.8 2.7 collective-permute-start.18
  (7 other events, 18.4 us)
Sparse Core Ops, SparseCore 0:
  66.7 106.3 all-gather.2
  174.7 57.3 all-gather.4
